TPU v7x, 32 devices: a whole 2x2x4 slice. The times are simulated.
32 devices in a mesh: ep: 8 (over z, core), tp: 4 (over y, x).
Axes of the slice: x: 2, y: 2, z: 4, core: 2. Of those that a mesh axis runs over, the one named last changes fastest.
Arguments:
- tokens: bfloat16 [128, 4096], P('ep', 'tp'), may hold values from -40 to 40
- norm_gain: bfloat16 [4096], P('tp'), may hold values from 0.099609375 to 1.8984375
- routes: int32 [128, 4], P('ep'), may hold values from 0 to 7, all different within a row; in each aligned block of 16 rows (0 to 15, 16 to 31, ...) at most 16 rows name the same one
- route_weights: float32 [128, 4], P('ep'), may hold values from 0.05 to 1
- w_gate: bfloat16 [8, 4096, 4096], P('ep', None, 'tp'), may hold values from -0.25 to 0.25
- w_up: bfloat16 [8, 4096, 4096], P('ep', None, 'tp'), may hold values from -0.25 to 0.25
- w_down: bfloat16 [8, 4096, 4096], P('ep', 'tp'), may hold values from -0.0234375 to 0.0234375
Outputs:
- mixed: bfloat16 [128, 4096], P('ep', 'tp')
Inputs may be any that keep to these rules, and one draw needn't show every extreme that they name: `routes`: within the 16 rows of one device, each token names 4 different experts, and no expert is named by more than 16 rows; some expert reaches 16.
All inputs are finite; a program needn't handle non-finite values.
Results may differ from a plain program's by a relative error of at most 0.018.
Values may be sent and summed in bfloat16 or wider, within the bound.
No kernel may reach another device: no remote copies, remote signals or barrier semaphores. Data moves between devices by JAX's collectives and lax.ppermute only.
A program may use at most 64 MiB of HBM per device.

v0:
```python
import jax
import jax.numpy as jnp
from jax import lax
from jax.sharding import PartitionSpec as P


def shards(tokens, norm_gain, routes, route_weights, w_gate, w_up, w_down):
    tok_rows = tokens.shape[0]
    topk = routes.shape[1]
    groups = lax.axis_size("ep")
    capacity = min(tok_rows, max(2, 2 * tok_rows * topk // groups))
    slot_rows = groups * capacity
    flat = routes.reshape(-1)
    order = jnp.arange(flat.shape[0], dtype=jnp.int32)
    earlier = (flat[:, None] == flat[None, :]) & (order[:, None] > order[None, :])
    slot = jnp.sum(earlier.astype(jnp.int32), axis=1)
    target = (flat * capacity + slot).reshape(tok_rows, topk)
    slot_ids = jnp.arange(slot_rows, dtype=jnp.int32)
    picker = jnp.any(target[None, :, :] == slot_ids[:, None, None], axis=2).astype(jnp.bfloat16)
    combine = jnp.sum(
        jnp.where(target[:, :, None] == slot_ids[None, None, :], route_weights[:, :, None], 0.0),
        axis=1,
    )
    whole, gain_whole = (
        lax.all_gather(tokens, "tp", axis=1, tiled=True),
        lax.all_gather(norm_gain.reshape(1, -1), "tp", axis=1, tiled=True),
    )
    full_values = whole.astype(jnp.float32)
    scale = lax.rsqrt(jnp.mean(full_values * full_values, axis=1, keepdims=True) + 1e-05)
    normed = (full_values * scale * gain_whole.astype(jnp.float32)).astype(jnp.bfloat16)
    outbound = jnp.dot(picker, normed, preferred_element_type=jnp.float32).astype(jnp.bfloat16)
    arrived = lax.all_to_all(
        outbound.reshape(groups, capacity, -1), "ep", split_axis=0, concat_axis=0, tiled=True
    ).reshape(slot_rows, -1)
    gate_pre = jnp.dot(arrived, w_gate[0], preferred_element_type=jnp.float32)
    up_pre = jnp.dot(arrived, w_up[0], preferred_element_type=jnp.float32)
    gated = jnp.minimum(gate_pre, 7.0)
    upper = jnp.clip(up_pre, -7.0, 7.0)
    hidden = ((upper + 1.0) * gated * jax.nn.sigmoid(1.702 * gated)).astype(jnp.bfloat16)
    partial_out = jnp.dot(hidden, w_down[0], preferred_element_type=jnp.float32).astype(
        jnp.bfloat16
    )
    summed = (
        lax.psum_scatter(partial_out, "tp", scatter_dimension=1, tiled=True)
        .astype(jnp.float32)
        .astype(jnp.bfloat16)
    )
    returned = lax.all_to_all(
        summed.reshape(groups, capacity, -1), "ep", split_axis=0, concat_axis=0, tiled=True
    ).reshape(slot_rows, -1)
    mixed = jnp.dot(combine, returned.astype(jnp.float32), precision=lax.Precision.HIGHEST)
    return mixed.astype(jnp.bfloat16)


def solution(mesh):
    placed = (
        P("ep", "tp"),
        P("tp"),
        P("ep", None),
        P("ep", None),
        P("ep", None, "tp"),
        P("ep", None, "tp"),
        P("ep", "tp", None),
    )
    return jax.shard_map(
        shards, mesh=mesh, in_specs=placed, out_specs=P("ep", "tp"), check_vma=False
    )
```

profile of v0, /device:TPU:0, one launch (start us, length us, event | category | flops | bytes accessed | tf_op | source)
XLA Modules:
  0.0 120.4 jit_solution(6978321878295605920)
XLA Ops:
  6.5 0.0 reduce-scatter.2.cloned.1.call-start
  6.5 10.1 %all_gather.6 = bf16[16,4096]{1,0:T(8,128)(2,1)S(1)} all-gather(bf16[16,1024]{1,0:T(8,128)(2,1)} %param.7), channel_id=1, replica_groups=mesh['ep'=8,'tp'=4] {'tp'}, dimensions={1}, use_global_device_ids=true | all-gather | bytes 163840 | tf_op jit(solution)/shard_map/all_gather | solution.py:25
  16.7 0.1 fusion.34
  16.8 0.8 copy.21
  17.6 0.1 eq.20
  17.7 0.2 convert_reduce_fusion
  17.9 0.1 reduce_sum.30
  17.9 0.1 copy.22
  18.0 0.7 multiply_add_fusion
  18.7 0.1 fusion.45
  18.8 7.9 %all-gather = bf16[4096]{0:T(1024)(128)(2,1)S(1)} all-gather(bf16[1024]{0:T(1024)(128)(2,1)} %param.8), channel_id=2, replica_groups=mesh['ep'=8,'tp'=4] {'tp'}, dimensions={0}, use_global_device_ids=true | all-gather | bytes 10240 | tf_op jit(solution)/shard_map/all_gather | solution.py:26
  26.7 0.5 convolution_convert_fusion
  27.2 31.2 %all_to_all.10 = bf16[8,16,4096]{2,1,0:T(8,128)(2,1)S(1)} all-to-all(bf16[8,16,4096]{2,1,0:T(8,128)(2,1)S(1)} %bitcast.36), channel_id=1, replica_groups=mesh['ep'=8,'tp'=4] {'ep'}, dimensions={0} | all-to-all | bytes 2097152 | tf_op jit(solution)/shard_map/all_to_all | solution.py:32
  58.4 4.6 %fusion.9 = f32[128,1024]{1,0:T(8,128)S(1)} fusion(bf16[128,4096]{1,0:T(8,128)(2,1)S(1)} %bitcast.34, bf16[1,4096,1024]{2,1,0:T(8,128)(2,1)} %param.11), kind=kOutput, calls=%fused_computation.8 | convolution fusion | flops 1073872896 | bytes 9961472 | tf_op jit(solution)/shard_map/dot_general | solution.py:35
  63.1 0.0 copy-start
  63.1 9.3 %fusion.6 = bf16[128,4096]{1,0:T(8,128)(2,1)} fusion(bf16[1,1024,4096]{2,1,0:T(8,128)(2,1)} %param.13, f32[128,1024]{1,0:T(8,128)S(1)} %fusion.9, bf16[128,4096]{1,0:T(8,128)(2,1)S(1)} %bitcast.35, bf16[1,4096,1024]{2,1,0:T(8,128)(2,1)} %param.12), kind=kOutput, calls=%fused_computation.6 | convolution fusion | flops 2149187584 | bytes 19398656 | tf_op jit(solution)/shard_map/dot_general | solution.py:40
  72.4 0.0 reduce-scatter.2.cloned.1.call-update
  72.4 26.0 %reduce-scatter.2.cloned.1.call-done = bf16[128,1024]{1,0:T(8,128)(2,1)} async-done(((bf16[128,4096]{1,0:T(8,128)(2,1)}), bf16[128,1024]{1,0:T(8,128)(2,1)}) %reduce-scatter.2.cloned.1.call-update) | async-done | bytes 262160 | tf_op jit(solution)/shard_map/reduce_scatter | solution.py:44
  98.4 4.6 %all-to-all-start.1 = ((bf16[8,16,1024]{2,1,0:T(8,128)(2,1)}), bf16[8,16,1024]{2,1,0:T(8,128)(2,1)S(1)}, u32[]{:S(2)}, u32[]{:S(2)}) async-start(bf16[8,16,1024]{2,1,0:T(8,128)(2,1)} %bitcast.38), calls=%async_computation.2 | async-start | bytes 524288 | tf_op jit(solution)/shard_map/all_to_all | solution.py:48
  103.0 0.0 copy-done
  103.1 0.1 select_reduce_fusion
  103.1 9.6 %all-to-all-done.1 = bf16[8,16,1024]{2,1,0:T(8,128)(2,1)S(1)} async-done(((bf16[8,16,1024]{2,1,0:T(8,128)(2,1)}), bf16[8,16,1024]{2,1,0:T(8,128)(2,1)S(1)}, u32[]{:S(2)}, u32[]{:S(2)}) %all-to-all-start.1) | async-done | bytes 262176 | tf_op jit(solution)/shard_map/all_to_all | solution.py:48
  112.8 0.8 convolution_convert_fusion.1
  (2 shorter events, 0.0 us)
Async XLA Ops:
  6.5 91.9 %reduce-scatter.2.cloned.1.call-start = ((), (), s32[]{:S(2)}) async-start(), calls=%async_computation.3 | async-start | bytes 1310720 | tf_op jit(solution)/shard_map/reduce_scatter | solution.py:44
  63.1 40.0 %copy-start = (f32[16,4]{0,1:T(4,128)S(1)}, f32[16,4]{0,1:T(4,128)}, u32[]{:S(2)}) copy-start(f32[16,4]{0,1:T(4,128)} %param.10) | copy-start | bytes 772
  98.4 14.3 %all-to-all-start.1 = ((bf16[8,16,1024]{2,1,0:T(8,128)(2,1)}), bf16[8,16,1024]{2,1,0:T(8,128)(2,1)S(1)}, u32[]{:S(2)}, u32[]{:S(2)}) async-start(bf16[8,16,1024]{2,1,0:T(8,128)(2,1)} %bitcast.38), calls=%async_computation.2 | async-start | bytes 524288 | tf_op jit(solution)/shard_map/all_to_all | solution.py:48
Sparse Core Ops, SparseCore 0:
  72.5 25.8 reduce-scatter.1
where the time goes:
time: 121 us; the launch traced here: 120 us
  blocking collectives  49.2 us (41%)
  waiting for transfers between devices  35.7 us (30%)
  matrix products  15.2 us (13%)
  between operations  13.4 us (11%)
  starting transfers between devices  4.62 us (4%)
    all_to_all x1, blocking collectives, shards(): lax.all_to_all(outbound.reshape(groups, capacity, -1), 'ep', split_axis=0...  31.2 us
    reduce_scatter x1, waiting for transfers between devices, shards(): lax.psum_scatter(partial_out, 'tp', scatter_dimension=1, tiled=True)  26 us
    all_gather x1, blocking collectives, shards(): lax.all_gather(tokens, 'tp', axis=1, tiled=True)  10.1 us
    all_to_all x1, waiting for transfers between devices, shards(): lax.all_to_all(summed.reshape(groups, capacity, -1), 'ep', split_axis=0,...  9.62 us
    dot_general x1, matrix products, shards(): jnp.dot(hidden, w_down[0], preferred_element_type=jnp.float32)  9.29 us
    all_gather x1, blocking collectives, shards(): lax.all_gather(norm_gain.reshape(1, -1), 'tp', axis=1, tiled=True)  7.86 us
    dot_general x1, matrix products, shards(): gate_pre = jnp.dot(arrived, w_gate[0], preferred_element_type=jnp.float32)  4.63 us
    all_to_all x1, starting transfers between devices, shards(): lax.all_to_all(summed.reshape(groups, capacity, -1), 'ep', split_axis=0,...  4.61 us
  transfers between devices with their start and end apart: 2, of which 2 were waited for; matrix products, arithmetic and copies ran while one was open for 0% of the time, Pallas kernels for 0%

commit v1 on v0

--- a/solution.py
+++ b/solution.py
@@ -23,7 +23,7 @@
     )
     whole, gain_whole = (
         lax.all_gather(tokens, "tp", axis=1, tiled=True),
-        lax.all_gather(norm_gain.reshape(1, -1), "tp", axis=1, tiled=True),
+        jnp.concatenate(lax.all_gather(norm_gain.reshape(1, -1), "tp"), axis=1),
     )
     full_values = whole.astype(jnp.float32)
     scale = lax.rsqrt(jnp.mean(full_values * full_values, axis=1, keepdims=True) + 1e-05)

time: 121 us -> 121 us (level)
  no operation moved by 1% of the time
where the time goes in v1:
time: 121 us; the launch traced here: 120 us
  blocking collectives  49.2 us (41%)
  waiting for transfers between devices  35.7 us (30%)
  matrix products  15.2 us (13%)
  between operations  13.4 us (11%)
  starting transfers between devices  4.62 us (4%)
    all_to_all x1, blocking collectives, shards(): lax.all_to_all(outbound.reshape(groups, capacity, -1), 'ep', split_axis=0...  31.2 us
    reduce_scatter x1, waiting for transfers between devices, shards(): lax.psum_scatter(partial_out, 'tp', scatter_dimension=1, tiled=True)  26 us
    all_gather x1, blocking collectives, shards(): lax.all_gather(tokens, 'tp', axis=1, tiled=True)  10.1 us
    all_to_all x1, waiting for transfers between devices, shards(): lax.all_to_all(summed.reshape(groups, capacity, -1), 'ep', split_axis=0,...  9.62 us
    dot_general x1, matrix products, shards(): jnp.dot(hidden, w_down[0], preferred_element_type=jnp.float32)  9.29 us
    all_gather x1, blocking collectives, shards(): lax.all_gather(norm_gain.reshape(1, -1), 'tp')  7.86 us
    dot_general x1, matrix products, shards(): gate_pre = jnp.dot(arrived, w_gate[0], preferred_element_type=jnp.float32)  4.63 us
    all_to_all x1, starting transfers between devices, shards(): lax.all_to_all(summed.reshape(groups, capacity, -1), 'ep', split_axis=0,...  4.61 us
  transfers between devices with their start and end apart: 2, of which 2 were waited for; matrix products, arithmetic and copies ran while one was open for 0% of the time, Pallas kernels for 0%

profile of v1, /device:TPU:0, one launch (start us, length us, event | category | flops | bytes accessed | tf_op | source)
XLA Modules:
  0.0 120.4 jit_solution(6978321878295605920)
XLA Ops:
  6.5 0.0 reduce-scatter.2.cloned.1.call-start
  6.5 10.1 %all_gather.6 = bf16[16,4096]{1,0:T(8,128)(2,1)S(1)} all-gather(bf16[16,1024]{1,0:T(8,128)(2,1)} %param.7), channel_id=1, replica_groups=mesh['ep'=8,'tp'=4] {'tp'}, dimensions={1}, use_global_device_ids=true | all-gather | bytes 163840 | tf_op jit(solution)/shard_map/all_gather | solution.py:25
  16.7 0.1 fusion.34
  16.8 0.8 copy.21
  17.6 0.1 eq.20
  17.7 0.2 convert_reduce_fusion
  17.9 0.1 reduce_sum.30
  17.9 0.1 copy.22
  18.0 0.7 multiply_add_fusion
  18.7 0.1 fusion.45
  18.8 7.9 %all-gather = bf16[4096]{0:T(1024)(128)(2,1)S(1)} all-gather(bf16[1024]{0:T(1024)(128)(2,1)} %param.8), channel_id=2, replica_groups=mesh['ep'=8,'tp'=4] {'tp'}, dimensions={0}, use_global_device_ids=true | all-gather | bytes 10240 | tf_op jit(solution)/shard_map/all_gather | solution.py:26
  26.7 0.5 convolution_convert_fusion
  27.2 31.2 %all_to_all.10 = bf16[8,16,4096]{2,1,0:T(8,128)(2,1)S(1)} all-to-all(bf16[8,16,4096]{2,1,0:T(8,128)(2,1)S(1)} %bitcast.36), channel_id=1, replica_groups=mesh['ep'=8,'tp'=4] {'ep'}, dimensions={0} | all-to-all | bytes 2097152 | tf_op jit(solution)/shard_map/all_to_all | solution.py:32
  58.4 4.6 %fusion.9 = f32[128,1024]{1,0:T(8,128)S(1)} fusion(bf16[128,4096]{1,0:T(8,128)(2,1)S(1)} %bitcast.34, bf16[1,4096,1024]{2,1,0:T(8,128)(2,1)} %param.11), kind=kOutput, calls=%fused_computation.8 | convolution fusion | flops 1073872896 | bytes 9961472 | tf_op jit(solution)/shard_map/dot_general | solution.py:35
  63.1 0.0 copy-start
  63.1 9.3 %fusion.6 = bf16[128,4096]{1,0:T(8,128)(2,1)} fusion(bf16[1,1024,4096]{2,1,0:T(8,128)(2,1)} %param.13, f32[128,1024]{1,0:T(8,128)S(1)} %fusion.9, bf16[128,4096]{1,0:T(8,128)(2,1)S(1)} %bitcast.35, bf16[1,4096,1024]{2,1,0:T(8,128)(2,1)} %param.12), kind=kOutput, calls=%fused_computation.6 | convolution fusion | flops 2149187584 | bytes 19398656 | tf_op jit(solution)/shard_map/dot_general | solution.py:40
  72.4 0.0 reduce-scatter.2.cloned.1.call-update
  72.4 26.0 %reduce-scatter.2.cloned.1.call-done = bf16[128,1024]{1,0:T(8,128)(2,1)} async-done(((bf16[128,4096]{1,0:T(8,128)(2,1)}), bf16[128,1024]{1,0:T(8,128)(2,1)}) %reduce-scatter.2.cloned.1.call-update) | async-done | bytes 262160 | tf_op jit(solution)/shard_map/reduce_scatter | solution.py:44
  98.4 4.6 %all-to-all-start.1 = ((bf16[8,16,1024]{2,1,0:T(8,128)(2,1)}), bf16[8,16,1024]{2,1,0:T(8,128)(2,1)S(1)}, u32[]{:S(2)}, u32[]{:S(2)}) async-start(bf16[8,16,1024]{2,1,0:T(8,128)(2,1)} %bitcast.38), calls=%async_computation.2 | async-start | bytes 524288 | tf_op jit(solution)/shard_map/all_to_all | solution.py:48
  103.0 0.0 copy-done
  103.1 0.1 select_reduce_fusion
  103.1 9.6 %all-to-all-done.1 = bf16[8,16,1024]{2,1,0:T(8,128)(2,1)S(1)} async-done(((bf16[8,16,1024]{2,1,0:T(8,128)(2,1)}), bf16[8,16,1024]{2,1,0:T(8,128)(2,1)S(1)}, u32[]{:S(2)}, u32[]{:S(2)}) %all-to-all-start.1) | async-done | bytes 262176 | tf_op jit(solution)/shard_map/all_to_all | solution.py:48
  112.8 0.8 convolution_convert_fusion.1
  (2 shorter events, 0.0 us)
Async XLA Ops:
  6.5 91.9 %reduce-scatter.2.cloned.1.call-start = ((), (), s32[]{:S(2)}) async-start(), calls=%async_computation.3 | async-start | bytes 1310720 | tf_op jit(solution)/shard_map/reduce_scatter | solution.py:44
  63.1 40.0 %copy-start = (f32[16,4]{0,1:T(4,128)S(1)}, f32[16,4]{0,1:T(4,128)}, u32[]{:S(2)}) copy-start(f32[16,4]{0,1:T(4,128)} %param.10) | copy-start | bytes 772
  98.4 14.3 %all-to-all-start.1 = ((bf16[8,16,1024]{2,1,0:T(8,128)(2,1)}), bf16[8,16,1024]{2,1,0:T(8,128)(2,1)S(1)}, u32[]{:S(2)}, u32[]{:S(2)}) async-start(bf16[8,16,1024]{2,1,0:T(8,128)(2,1)} %bitcast.38), calls=%async_computation.2 | async-start | bytes 524288 | tf_op jit(solution)/shard_map/all_to_all | solution.py:48
Sparse Core Ops, SparseCore 0:
  72.5 25.8 reduce-scatter.1
